TPU v7x, 256 devices: a 4x2x16 block of a 4x16x16 slice. The times are simulated.
256 devices in a mesh: grp: 2 (over y), sp: 32 (over z, core), tp: 4 (over x).
Axes of the slice: x: 4, y: 2, z: 16, core: 2. Of those that a mesh axis runs over, the one named last changes fastest.
The devices are a block of a 4x16x16 slice.
Arguments:
- query_wide: bfloat16 [32768, 1024], P(('grp', 'sp'), 'tp'), parts along dimension 0, may hold values from -6 to 6
- key_wide: bfloat16 [32768, 1024], P(('grp', 'sp'), 'tp'), parts along dimension 0, may hold values from -6 to 6
- value_wide: bfloat16 [32768, 1024], P(('grp', 'sp'), 'tp'), parts along dimension 0, may hold values from -6 to 6
- decay_wide: float32 [32768, 8], P(('grp', 'sp'), 'tp'), parts along dimension 0, may hold values from -2 to 0, as said below
- query_narrow: bfloat16 [32768, 1024], P(('grp', 'sp'), 'tp'), parts along dimension 0, may hold values from -6 to 6
- key_narrow: bfloat16 [32768, 1024], P(('grp', 'sp'), 'tp'), parts along dimension 0, may hold values from -6 to 6
- value_narrow: bfloat16 [32768, 1024], P(('grp', 'sp'), 'tp'), parts along dimension 0, may hold values from -6 to 6
- decay_narrow: float32 [32768, 16], P(('grp', 'sp'), 'tp'), parts along dimension 0, may hold values from -2 to 0, as said below
- residual: bfloat16 [32768, 2048], P(('grp', 'sp', 'tp')), parts along dimension 0, may hold values from -6 to 6
- out_wide: bfloat16 [1024, 2048], P('tp'), may hold values from -0.125 to 0.125
- out_narrow: bfloat16 [1024, 2048], P('tp'), may hold values from -0.125 to 0.125
- norm_gain: float32 [2048], replicated, may hold values from 0.1 to 1.9
- routes: int32 [32768, 2], P(('grp', 'sp', 'tp')), parts along dimension 0, may hold values from 0 to 31, all different within a row; in each aligned block of 128 rows (0 to 127, 128 to 255, ...) at most 12 rows name the same one
- route_weights: float32 [32768, 2], P(('grp', 'sp', 'tp')), parts along dimension 0, may hold values from 0.1 to 1
- expert_gate: bfloat16 [32, 2048, 2048], P('sp', None, 'tp'), may hold values from -0.375 to 0.375
- expert_up: bfloat16 [32, 2048, 2048], P('sp', None, 'tp'), may hold values from -0.375 to 0.375
- expert_down: bfloat16 [32, 2048, 2048], P('sp', 'tp'), may hold values from -0.03125 to 0.03125
Outputs:
- layer_out: bfloat16 [32768, 2048], P(('grp', 'sp', 'tp')), parts along dimension 0
There are 2 independent parts, one for each index of `grp`. A program takes and returns all parts, laid end to end along the dimension named above; an argument that names none is the same for every part. Nothing has to cross between parts.
Inputs may be any that keep to these rules, and one draw needn't show every extreme that they name: `decay_wide`: every entry is negative. `decay_narrow`: every entry is negative. `routes`: each row names 2 different experts; on the rows of one device no expert is named more than 12 times, a bound that some block reaches.
All inputs are finite; a program needn't handle non-finite values.
Results may differ from a plain program's by a relative error of at most 0.018.
Values may be sent and summed in bfloat16 or wider, within the bound.
No kernel may reach another device: no remote copies, remote signals or barrier semaphores. Data moves between devices by JAX's collectives and lax.ppermute only.
A program may use at most 128 MiB of HBM per device.

v0:
```python
import jax
import jax.numpy as jnp
from jax import lax
from jax.sharding import Mesh
from jax.sharding import PartitionSpec as P

HEAD_WIDE = 128
HEAD_NARROW = 64
TOP_K = 2
SP = ("sp_0", "sp_1")
GRP_SP = ("grp", "sp_0", "sp_1")
GRP_SP_TP = ("grp", "sp_0", "sp_1", "tp")
norm_eps = 1e-05
clamp_limit = 7.0
swish_alpha = 1.702
rotary_base = 10000.0


def filled_with(value, identity):
    return jax.tree.map(
        lambda a, e: jnp.broadcast_to(jnp.asarray(e, a.dtype), a.shape), value, identity
    )


def prefix_by_axis(value, axes, combine, identity):
    before = start = filled_with(value, identity)
    total = value
    for axis in reversed(axes):
        length, mine = (lax.axis_size(axis), lax.axis_index(axis))
        pieces = jax.tree.map(
            lambda part, kind: lax.all_gather(part.astype(kind), axis),
            total,
            jax.tree.map(lambda a: jnp.bfloat16 if a.dtype == jnp.float32 else a.dtype, value),
        )
        inside, total = (start, start)
        for k in range(length):
            passed = k < mine
            total = combine(
                total, jax.tree.map(lambda part, own: part[k].astype(own.dtype), pieces, value)
            )
            inside = jax.tree.map(lambda new, old: jnp.where(passed, new, old), total, inside)
        before = combine(inside, before)
    return before


def cut_along(value, dim, length):
    lengths = value.shape
    pieces = value.reshape(*lengths[:dim], length, lengths[dim] // length, *lengths[dim + 1 :])
    return jnp.moveaxis(pieces, dim, 0)


def sent_and_summed(value, axis, dim):
    pieces = cut_along(value, dim, lax.axis_size(axis))
    arrived = lax.all_to_all(pieces, axis, split_axis=0, concat_axis=0, tiled=True)
    return arrived.astype(jnp.float32).sum(axis=0)


def laid_out(pieces, dim):
    pieces = jnp.moveaxis(pieces, 0, dim)
    lengths = pieces.shape
    return pieces.reshape(*lengths[:dim], lengths[dim] * lengths[dim + 1], *lengths[dim + 2 :])


def turned_blocks(pieces, axes, order):
    inside = pieces.shape[1:]
    filled = pieces.reshape(*(lax.axis_size(a) for a in axes), *inside)
    for k in order:
        filled = lax.all_to_all(filled, axes[k], k, k, tiled=True)
    return filled.reshape(-1, *inside)


def core_and_chips(value, groups, order, split_dim, concat_dim):
    length = lax.axis_size(groups[0]) * lax.axis_size(groups[1])
    pieces = cut_along(value, split_dim, length)
    return laid_out(turned_blocks(pieces, groups, order), concat_dim)


def rotate(values, positions):
    half_width = values.shape[-1] // 2
    inverse = rotary_base ** (-jnp.arange(half_width, dtype=jnp.float32) / half_width)
    angles = positions[:, None] * inverse[None, :]
    cosine = jnp.cos(angles)[:, None, :]
    sine_part = jnp.sin(angles)[:, None, :]
    lower_half = values[..., :half_width]
    upper_half = values[..., half_width:]
    return jnp.concatenate(
        [
            lower_half * cosine - upper_half * sine_part,
            lower_half * sine_part + upper_half * cosine,
        ],
        axis=-1,
    )


def group_norm(output_heads):
    center = jnp.mean(output_heads, axis=-1, keepdims=True)
    spread = jnp.mean(jnp.square(output_heads - center), axis=-1, keepdims=True)
    return (output_heads - center) * lax.rsqrt(spread + norm_eps)


def local_terms(query_in, key_in, value_in, log_decay, head_width, positions):
    length = query_in.shape[0]
    attention_group_count = query_in.shape[1] // head_width
    query_heads = query_in.astype(jnp.float32).reshape(length, attention_group_count, head_width)
    key_heads = key_in.astype(jnp.float32).reshape(length, attention_group_count, head_width)
    query_f = rotate(query_heads, positions).astype(jnp.bfloat16).astype(jnp.float32)
    key_f = (
        (rotate(key_heads, positions) * head_width ** (-0.5))
        .astype(jnp.bfloat16)
        .astype(jnp.float32)
    )
    value_f = value_in.reshape(length, attention_group_count, head_width).astype(jnp.float32)
    cumulative = jnp.cumsum(log_decay, axis=0)
    steps_in = jnp.arange(length, dtype=jnp.int32)
    causal = steps_in[:, None] >= steps_in[None, :]
    gaps = cumulative.T[:, :, None] - cumulative.T[:, None, :]
    decay_grid = jnp.exp(jnp.where(causal[None], gaps, -jnp.inf))
    scores = jnp.einsum("thd,shd->hts", query_f, key_f) * decay_grid
    inner_part = jnp.einsum("hts,she->the", scores, value_f)
    total_log = cumulative[-1]
    weighted = key_f * jnp.exp(total_log[None, :] - cumulative)[:, :, None]
    state_local = jnp.einsum("shd,she->hde", weighted, value_f)
    return (query_f, cumulative, inner_part, total_log, state_local)


def finish(parts, state_in):
    query_f, cumulative, inner_part = (parts[0], parts[1], parts[2])
    carried_part = jnp.exp(cumulative)[:, :, None] * jnp.einsum("thd,hde->the", query_f, state_in)
    normed_heads = group_norm(inner_part + carried_part)
    return normed_heads.reshape(normed_heads.shape[0], -1).astype(jnp.bfloat16)


def combine(earlier, later):
    return (
        earlier[0] + later[0],
        jnp.exp(later[0])[:, None, None] * earlier[1] + later[1],
        earlier[2] + later[2],
        jnp.exp(later[2])[:, None, None] * earlier[3] + later[3],
    )


def activate(gate_pre, up_pre):
    gate_clip = jnp.minimum(gate_pre, clamp_limit)
    up_clip = jnp.clip(up_pre, -clamp_limit, clamp_limit)
    return gate_clip * jax.nn.sigmoid(swish_alpha * gate_clip) * (up_clip + 1.0)


def body(
    query_wide,
    key_wide,
    value_wide,
    decay_wide,
    query_narrow,
    key_narrow,
    value_narrow,
    decay_narrow,
    residual,
    out_wide,
    out_narrow,
    norm_gain,
    routes,
    route_weights,
    expert_gate,
    expert_up,
    expert_down,
):
    length = query_wide.shape[0]
    tp_count = lax.axis_size("tp")
    experts = lax.axis_size(SP)
    model_width = residual.shape[1]
    positions = (lax.axis_index(SP) * length + jnp.arange(length, dtype=jnp.int32)).astype(
        jnp.float32
    )
    wide_parts = local_terms(query_wide, key_wide, value_wide, decay_wide, HEAD_WIDE, positions)
    narrow_parts = local_terms(
        query_narrow, key_narrow, value_narrow, decay_narrow, HEAD_NARROW, positions
    )
    local_states = (wide_parts[3], wide_parts[4], narrow_parts[3], narrow_parts[4])
    identity = tuple((jnp.zeros_like(member) for member in local_states))
    carried = prefix_by_axis(local_states, SP, combine, identity)
    mixed_wide = finish(wide_parts, carried[1])
    mixed_narrow = finish(narrow_parts, carried[3])
    rows_dev = length // tp_count
    attention = sent_and_summed(
        (
            jnp.dot(mixed_wide, out_wide, preferred_element_type=jnp.float32)
            + jnp.dot(mixed_narrow, out_narrow, preferred_element_type=jnp.float32)
        ).astype(jnp.bfloat16),
        "tp",
        0,
    )
    hidden_state = residual.astype(jnp.float32) + attention
    scale_row = lax.rsqrt(jnp.mean(hidden_state * hidden_state, axis=-1, keepdims=True) + norm_eps)
    normed = (hidden_state * scale_row * norm_gain).astype(jnp.bfloat16)
    capacity = max(2, 3 * rows_dev * TOP_K // (2 * experts))
    flat_expert = routes.reshape(-1)
    one_hot = (flat_expert[:, None] == jnp.arange(experts, dtype=jnp.int32)[None, :]).astype(
        jnp.int32
    )
    rank_in = jnp.sum((jnp.cumsum(one_hot, axis=0) - one_hot) * one_hot, axis=1)
    slot_index = flat_expert * capacity + rank_in
    source_row = jnp.arange(rows_dev * TOP_K, dtype=jnp.int32) // TOP_K
    slot_table = jnp.zeros((experts * capacity,), jnp.int32).at[slot_index].set(source_row + 1)
    padded = jnp.concatenate([jnp.zeros((1, model_width), jnp.bfloat16), normed], axis=0)
    send_slots = padded[slot_table].reshape(experts, capacity, model_width)
    gate_shard = expert_gate[0]
    up_shard = expert_up[0]
    down_shard = expert_down[0]
    gathered = lax.all_gather(
        core_and_chips(send_slots, ("sp_0", "sp_1"), (1, 0), 0, 0), "tp", axis=0, tiled=True
    )
    flat_rows = gathered.reshape(-1, model_width)
    gate_pre = jnp.dot(flat_rows, gate_shard, preferred_element_type=jnp.float32)
    up_pre = jnp.dot(flat_rows, up_shard, preferred_element_type=jnp.float32)
    hidden = activate(gate_pre, up_pre).astype(jnp.bfloat16)
    partial_value = jnp.dot(hidden, down_shard, preferred_element_type=jnp.float32)
    partial_value = partial_value.reshape(gathered.shape[0], gathered.shape[1], model_width)
    summed = sent_and_summed(
        partial_value.reshape(tp_count, experts, capacity, model_width).astype(jnp.bfloat16),
        "tp",
        0,
    )
    expert_output = summed.reshape(experts, capacity, model_width).astype(jnp.bfloat16)
    returned = lax.all_to_all(expert_output, SP, split_axis=0, concat_axis=0, tiled=True)
    picked = returned.reshape(experts * capacity, model_width)[slot_index].astype(jnp.float32)
    routed = jnp.sum(
        (picked * route_weights.reshape(-1)[:, None]).reshape(rows_dev, TOP_K, model_width), axis=1
    )
    return (hidden_state + routed).astype(jnp.bfloat16)


def solution(mesh):
    torus = Mesh(
        mesh.devices.reshape(mesh.shape["grp"], 16, 2, mesh.shape["tp"]),
        ("grp", "sp_0", "sp_1", "tp"),
    )
    in_specs = (
        P(GRP_SP, "tp"),
        P(GRP_SP, "tp"),
        P(GRP_SP, "tp"),
        P(GRP_SP, "tp"),
        P(GRP_SP, "tp"),
        P(GRP_SP, "tp"),
        P(GRP_SP, "tp"),
        P(GRP_SP, "tp"),
        P(GRP_SP_TP, None),
        P("tp", None),
        P("tp", None),
        P(),
        P(GRP_SP_TP, None),
        P(GRP_SP_TP, None),
        P(SP, None, "tp"),
        P(SP, None, "tp"),
        P(SP, "tp", None),
    )
    out_specs = P(GRP_SP_TP, None)
    return jax.shard_map(body, mesh=torus, in_specs=in_specs, out_specs=out_specs, check_vma=False)
```

profile of v0, /device:TPU:33, one launch (start us, length us, event | category | flops | bytes accessed | tf_op | source)
XLA Modules:
  0.0 619.4 jit_solution(2552972941295234430)
XLA Ops:
  11.3 1.1 copy.218
  12.5 1.1 copy.189
  14.4 1.9 copy.219
  16.3 1.9 copy.220
  19.9 2.4 subtract_convert_fusion
  23.0 22.0 %all-gather = bf16[4,128,128]{2,1,0:T(8,128)(2,1)S(1)} all-gather(bf16[2,128,128]{2,1,0:T(8,128)(2,1)S(1)} %convolution_convert_fusion.1), channel_id=2, replica_groups=mesh['grp'=2,'sp_0'=16,'sp_1'=2,'tp'=4] {'sp_1'}, dimensions={0}, use_global_device_ids=true | all-gather | bytes 196608 | tf_op jit(solution)/shard_map/all_gather | solution.py:31
  45.0 1.8 all-gather.2
  48.3 1.2 reduce-window.24
  54.2 1.8 multiply_subtract_fusion.1
  56.2 2.0 all-gather.1
  58.2 2.0 all-gather.4
  60.3 32.4 %all_gather.48 = bf16[16,4,64,64]{3,2,1,0:T(8,128)(2,1)S(1)} all-gather(bf16[1,4,64,64]{3,2,1,0:T(8,128)(2,1)S(1)} %fusion.70), channel_id=1, replica_groups=mesh['grp'=2,'sp_0'=16,'sp_1'=2,'tp'=4] {'sp_0'}, dimensions={0}, use_global_device_ids=true | all-gather | bytes 557056 | tf_op jit(solution)/shard_map/all_gather | solution.py:31
  92.8 21.5 %all-gather.5 = bf16[16,1,4]{2,1,0:T(2,128)(2,1)S(1)} all-gather(bf16[1,1,4]{2,1,0:T(2,128)(2,1)S(1)} %get-tuple-element.65), channel_id=1, replica_groups=mesh['grp'=2,'sp_0'=16,'sp_1'=2,'tp'=4] {'sp_0'}, dimensions={0}, use_global_device_ids=true | all-gather | bytes 136 | tf_op jit(solution)/shard_map/all_gather | solution.py:31
  115.0 19.9 %all-gather.3 = bf16[16,1,2]{2,1,0:T(2,128)(2,1)S(1)} all-gather(bf16[1,1,2]{2,1,0:T(2,128)(2,1)} %get-tuple-element.68), channel_id=1, replica_groups=mesh['grp'=2,'sp_0'=16,'sp_1'=2,'tp'=4] {'sp_0'}, dimensions={0}, use_global_device_ids=true | all-gather | bytes 68 | tf_op jit(solution)/shard_map/all_gather | solution.py:31
  136.3 4.1 fusion.31
  140.4 1.8 fusion.327
  142.6 3.1 fusion.34
  145.7 2.5 fusion.326
  148.3 2.0 fusion.328
  150.4 2.0 add_convert_fusion
  152.4 4.7 all-to-all-start
  158.8 1.4 scatter_custom_fusion
  160.2 12.2 %all-to-all-done = bf16[4,128,2048]{2,1,0:T(8,128)(2,1)} async-done(((bf16[4,128,2048]{2,1,0:T(8,128)(2,1)}), bf16[4,128,2048]{2,1,0:T(8,128)(2,1)}, u32[]{:S(2)}, u32[]{:S(2)}) %all-to-all-start) | async-done | bytes 2097184 | tf_op jit(solution)/shard_map/all_to_all | solution.py:54
  172.4 2.1 convert_reduce_fusion
  175.9 3.1 gather_fusion
  179.0 3.6 reshape_reshape_reshape.3
  182.6 2.5 copy.204
  185.1 24.8 %all_to_all.25 = bf16[16,2,1,12,2048]{4,0,3,2,1:T(8,128)(2,1)S(1)} all-to-all(bf16[16,2,1,12,2048]{4,0,3,2,1:T(8,128)(2,1)S(1)} %copy.204), channel_id=1, replica_groups=mesh['grp'=2,'sp_0'=16,'sp_1'=2,'tp'=4] {'sp_1'}, dimensions={1} | all-to-all | bytes 3145728 | tf_op jit(solution)/shard_map/all_to_all | solution.py:68
  209.9 1.6 copy.205
  211.5 72.3 %all_to_all.26 = bf16[16,2,1,12,2048]{4,1,3,2,0:T(2,128)(2,1)S(1)} all-to-all(bf16[16,2,1,12,2048]{4,1,3,2,0:T(2,128)(2,1)S(1)} %copy.205), channel_id=1, replica_groups=mesh['grp'=2,'sp_0'=16,'sp_1'=2,'tp'=4] {'sp_0'}, dimensions={0} | all-to-all | bytes 3145728 | tf_op jit(solution)/shard_map/all_to_all | solution.py:68
  283.8 2.6 copy.206
  286.4 3.7 reshape_reshape.4
  290.1 72.6 %all-gather.11.cloned.1.call-done = bf16[128,12,2048]{2,0,1:T(8,128)(2,1)} async-done(((bf16[32,12,2048]{2,0,1:T(8,128)(2,1)}), bf16[128,12,2048]{2,0,1:T(8,128)(2,1)}) %all-gather.11.cloned.1.call-update) | async-done | bytes 6291472 | tf_op jit(solution)/shard_map/all_gather | solution.py:209
  362.7 9.7 %copy.207 = bf16[128,12,2048]{2,1,0:T(8,128)(2,1)} copy(bf16[128,12,2048]{2,0,1:T(8,128)(2,1)} %all-gather.11.cloned.1.call-done) | data formatting | bytes 12582912 | tf_op jit(solution)/shard_map/all_gather | solution.py:209
  372.3 10.7 %reshape.746 = bf16[1536,2048]{1,0:T(8,128)(2,1)} reshape(bf16[128,12,2048]{2,1,0:T(8,128)(2,1)} %copy.207) | data formatting | bytes 12582912 | tf_op jit(solution)/shard_map/reshape | solution.py:212
  383.1 6.3 %convolution_minimum_fusion = f32[1536,512]{1,0:T(8,128)S(1)} fusion(bf16[1536,2048]{1,0:T(8,128)(2,1)} %reshape.746, bf16[1,2048,512]{2,1,0:T(8,128)(2,1)} %param.31), kind=kOutput, calls=%fused_computation.13 | convolution fusion | flops 3222011904 | bytes 11534336 | tf_op jit(solution)/shard_map/dot_general | solution.py:213
  389.4 5.0 fusion.7
  394.4 3.6 dot_general.53
  398.0 6.1 convert_bitcast_fusion
  404.1 73.7 %all_to_all.27 = bf16[4,1,32,12,2048]{4,2,3,1,0:T(8,128)(2,1)S(1)} all-to-all(bf16[4,1,32,12,2048]{4,2,3,1,0:T(8,128)(2,1)S(1)} %convert_bitcast_fusion), channel_id=1, replica_groups=mesh['grp'=2,'sp_0'=16,'sp_1'=2,'tp'=4] {'tp'}, dimensions={0} | all-to-all | bytes 12582912 | tf_op jit(solution)/shard_map/all_to_all | solution.py:54
  477.9 1.2 bitcast_reduce_fusion
  479.1 2.2 copy.211
  481.3 14.4 %all-to-all-start.4 = ((bf16[32,12,2048]{2,1,0:T(8,128)(2,1)}), bf16[32,12,2048]{2,1,0:T(8,128)(2,1)}, u32[]{:S(2)}, u32[]{:S(2)}) async-start(bf16[32,12,2048]{2,1,0:T(8,128)(2,1)} %copy.211), calls=%async_computation.4 | async-start | bytes 4194304 | tf_op jit(solution)/shard_map/all_to_all | solution.py:224
  495.9 98.6 %all-to-all-done.4 = bf16[32,12,2048]{2,1,0:T(8,128)(2,1)} async-done(((bf16[32,12,2048]{2,1,0:T(8,128)(2,1)}), bf16[32,12,2048]{2,1,0:T(8,128)(2,1)}, u32[]{:S(2)}, u32[]{:S(2)}) %all-to-all-start.4) | async-done | bytes 1572896 | tf_op jit(solution)/shard_map/all_to_all | solution.py:224
  594.4 3.6 reshape.748
  598.0 4.9 gather_fusion.1
  603.0 3.4 reshape.793
  606.4 4.9 multiply_reduce_fusion
  (143 shorter events, 20.9 us)
Async XLA Ops:
  6.5 391.5 %copy-start = (bf16[1,512,2048]{2,1,0:T(8,128)(2,1)S(1)}, bf16[1,512,2048]{2,1,0:T(8,128)(2,1)}, u32[]{:S(2)}) copy-start(bf16[1,512,2048]{2,1,0:T(8,128)(2,1)} %param.33) | copy-start | bytes 6291460
  6.6 136.0 %all-gather.9.cloned.1.call-start = ((), (), s32[]{:S(2)}) async-start(), calls=%async_computation.5 | async-start | bytes 1114112 | tf_op jit(solution)/shard_map/all_gather | solution.py:31
  8.4 0.6 copy-start.21
  19.9 2.6 copy-start.32
  22.3 26.0 %copy-start.18 = (f32[512,4]{0,1:T(4,128)S(1)}, f32[512,4]{0,1:T(4,128)}, u32[]{:S(2)}) copy-start(f32[512,4]{0,1:T(4,128)} %param.24) | copy-start | bytes 24580
  22.3 29.9 %copy-start.6 = (bf16[512,256]{1,0:T(8,128)(2,1)S(1)}, bf16[512,256]{1,0:T(8,128)(2,1)}, u32[]{:S(2)}) copy-start(bf16[512,256]{1,0:T(8,128)(2,1)} %param.21) | copy-start | bytes 786436
  22.3 30.0 %copy-start.7 = (bf16[512,256]{1,0:T(8,128)(2,1)S(1)}, bf16[512,256]{1,0:T(8,128)(2,1)}, u32[]{:S(2)}) copy-start(bf16[512,256]{1,0:T(8,128)(2,1)} %param.22) | copy-start | bytes 786436
  22.5 29.6 %copy-start.10 = (bf16[512,2,128]{2,0,1:T(8,128)(2,1)}, bf16[512,2,128]{2,0,1:T(8,128)(2,1)S(1)}, u32[]{:S(2)}) copy-start(bf16[512,2,128]{2,0,1:T(8,128)(2,1)S(1)} %fusion.41) | copy-start | bytes 786436
  46.8 1.4 copy-start.23
  47.4 0.8 copy-start.27
  47.4 2.4 copy-start.25
  49.9 0.6 copy-start.15
  53.5 2.5 copy-start.13
  54.2 82.1 %copy-start.16 = (f32[1,4,4,128]{3,1,2,0:T(4,128)S(1)}, f32[1,4,4,128]{3,1,2,0:T(4,128)}, u32[]{:S(2)}) copy-start(f32[1,4,4,128]{3,1,2,0:T(4,128)} %copy-done.15) | copy-start | bytes 24580
  56.0 4.3 copy-start.11
  56.0 4.4 copy-start.12
  60.2 76.1 %copy-start.28 = (f32[4]{0:T(128)}, f32[4]{0:T(128)S(1)}, u32[]{:S(2)}) copy-start(f32[4]{0:T(128)S(1)} %get-tuple-element.66) | copy-start | bytes 52
  60.2 76.0 %copy-start.29 = (f32[4]{0:T(128)}, f32[4]{0:T(128)S(1)}, u32[]{:S(2)}) copy-start(f32[4]{0:T(128)S(1)} %get-tuple-element.67) | copy-start | bytes 52
  136.3 4.1 copy-start.14
  140.4 2.0 copy-start.24
  140.4 2.2 copy-start.20
  140.4 2.2 copy-start.26
  142.4 3.2 copy-start.8
  142.4 3.2 copy-start.9
  142.5 3.2 copy-start.22
  148.3 2.1 copy-start.5
  152.4 4.8 copy-start.19
  152.4 20.0 %all-to-all-start = ((bf16[4,128,2048]{2,1,0:T(8,128)(2,1)}), bf16[4,128,2048]{2,1,0:T(8,128)(2,1)}, u32[]{:S(2)}, u32[]{:S(2)}) async-start(bf16[4,128,2048]{2,1,0:T(8,128)(2,1)} %bitcast.468), calls=%async_computation | async-start | bytes 4194304 | tf_op jit(solution)/shard_map/all_to_all | solution.py:54
  157.1 17.5 %copy-start.4 = (bf16[128,2048]{1,0:T(8,128)(2,1)S(1)}, bf16[128,2048]{1,0:T(8,128)(2,1)}, u32[]{:S(2)}) copy-start(bf16[128,2048]{1,0:T(8,128)(2,1)} %param.25) | copy-start | bytes 1572868
  157.1 205.6 %all-gather.11.cloned.1.call-start = ((), (), s32[]{:S(2)}) async-start(), calls=%async_computation.6 | async-start | bytes 7864320 | tf_op jit(solution)/shard_map/all_gather | solution.py:209
  160.2 15.3 %copy-start.17 = (f32[2048]{0:T(1024)S(1)}, f32[2048]{0:T(1024)}, u32[]{:S(2)}) copy-start(f32[2048]{0:T(1024)} %param.28) | copy-start | bytes 24580
  174.6 1.0 copy-start.1
  383.1 6.3 %copy-start.3 = (bf16[1536,2048]{1,0:T(8,128)(2,1)S(1)}, bf16[1536,2048]{1,0:T(8,128)(2,1)}, u32[]{:S(2)}) copy-start(bf16[1536,2048]{1,0:T(8,128)(2,1)} %reshape.746) | copy-start | bytes 18874372
  383.1 6.3 %copy-start.31 = (bf16[1,2048,512]{2,1,0:T(8,128)(2,1)S(1)}, bf16[1,2048,512]{2,1,0:T(8,128)(2,1)}, u32[]{:S(2)}) copy-start(bf16[1,2048,512]{2,1,0:T(8,128)(2,1)} %param.32) | copy-start | bytes 6291460
  481.3 14.4 %copy-start.30 = (f32[128,2]{0,1:T(2,128)S(1)}, f32[128,2]{0,1:T(2,128)}, u32[]{:S(2)}) copy-start(f32[128,2]{0,1:T(2,128)} %param.30) | copy-start | bytes 3076
  481.3 113.1 %all-to-all-start.4 = ((bf16[32,12,2048]{2,1,0:T(8,128)(2,1)}), bf16[32,12,2048]{2,1,0:T(8,128)(2,1)}, u32[]{:S(2)}, u32[]{:S(2)}) async-start(bf16[32,12,2048]{2,1,0:T(8,128)(2,1)} %copy.211), calls=%async_computation.4 | async-start | bytes 4194304 | tf_op jit(solution)/shard_map/all_to_all | solution.py:224
  606.4 4.9 copy-start.2
Sparse Core Ops, SparseCore 0:
  48.3 54.4 all-gather.8
  290.2 72.4 all-gather.10
where the time goes:
time: 626 us; the launch traced here: 619 us
  blocking collectives  273 us (44%)
  waiting for transfers between devices  184 us (29%)
  local copies, waits for them, and re-layouts  72.1 us (12%)
  matrix products  33.7 us (5%)
  other arithmetic  24.1 us (4%)
  starting transfers between devices  19.1 us (3%)
  between operations  14.3 us (2%)
    all_gather x7, blocking collectives, prefix_by_axis(): lax.all_gather(part.astype(kind), axis)  102 us
    all_to_all x1, waiting for transfers between devices, body(): lax.all_to_all(expert_output, SP, split_axis=0, concat_axis=0, tiled=True)  98.6 us
    all_to_all x2, blocking collectives, turned_blocks(): filled = lax.all_to_all(filled, axes[k], k, k, tiled=True)  97.1 us
    all_to_all x1, blocking collectives, sent_and_summed(): lax.all_to_all(pieces, axis, split_axis=0, concat_axis=0, tiled=True)  73.7 us
    all_gather x1, waiting for transfers between devices, body(): lax.all_gather(core_and_chips(send_slots, ('sp_0', 'sp_1'), (1, 0), 0, 0)...  72.6 us
    all_to_all x1, starting transfers between devices, body(): lax.all_to_all(expert_output, SP, split_axis=0, concat_axis=0, tiled=True)  14.4 us
  transfers between devices with their start and end apart: 4, of which 3 were waited for; matrix products, arithmetic and copies ran while one was open for 3% of the time, Pallas kernels for 0%

commit v1 on v0

--- a/solution.py
+++ b/solution.py
@@ -14,6 +14,11 @@
 clamp_limit = 7.0
 swish_alpha = 1.702
 rotary_base = 10000.0
+
+
+def gather_by_exchange(value, axis, dim):
+    copies = jnp.concatenate([value] * lax.axis_size(axis), axis=dim)
+    return lax.all_to_all(copies, axis, dim, dim, tiled=True)
 
 
 def filled_with(value, identity):
@@ -206,8 +211,8 @@
     gate_shard = expert_gate[0]
     up_shard = expert_up[0]
     down_shard = expert_down[0]
-    gathered = lax.all_gather(
-        core_and_chips(send_slots, ("sp_0", "sp_1"), (1, 0), 0, 0), "tp", axis=0, tiled=True
+    gathered = gather_by_exchange(
+        core_and_chips(send_slots, ("sp_0", "sp_1"), (1, 0), 0, 0), "tp", 0
     )
     flat_rows = gathered.reshape(-1, model_width)
     gate_pre = jnp.dot(flat_rows, gate_shard, preferred_element_type=jnp.float32)

time: 626 us -> 659 us (1.053)
  blocking collectives: 273 us -> 359 us
  waiting for transfers between devices: 184 us -> 111 us
  starting transfers between devices: 19.1 us -> 34.5 us
    all_to_all x0 -> x1, blocking collectives: none -> 94.2 us  [gather_by_exchange(): return lax.all_to_all(copies, axis, dim, dim, tiled=True)]
    all_gather x1 -> x0, waiting for transfers between devices: 72.6 us -> none  [body(): lax.all_gather(core_and_chips(send_slots, ('sp_0', 'sp_1'), (1, 0), 0, 0)...]
    all_to_all x1, starting transfers between devices: 14.4 us -> 29.9 us  [body(): lax.all_to_all(expert_output, SP, split_axis=0, concat_axis=0, tiled=True)]
    all_gather x1 -> x0, local copies, waits for them, and re-layouts: 9.65 us -> none  [body(): lax.all_gather(core_and_chips(send_slots, ('sp_0', 'sp_1'), (1, 0), 0, 0)...]
    all_to_all x1, blocking collectives: 73.7 us -> 65.9 us  [sent_and_summed(): lax.all_to_all(pieces, axis, split_axis=0, concat_axis=0, tiled=True)]
    concatenate x0 -> x1, local copies, waits for them, and re-layouts: none -> 6.84 us  [gather_by_exchange(): copies = jnp.concatenate([value] * lax.axis_size(axis), axis=dim)]
  transfers between devices with their start and end apart: 4 -> 3, of which waited for: 3 -> 2; matrix products, arithmetic and copies ran while one was open for 3% -> 3% of each run, Pallas kernels for 0% -> 0%
where the time goes in v1:
time: 659 us; the launch traced here: 652 us
  blocking collectives  359 us (54%)
  waiting for transfers between devices  111 us (17%)
  local copies, waits for them, and re-layouts  71.1 us (11%)
  starting transfers between devices  34.5 us (5%)
  matrix products  33.7 us (5%)
  other arithmetic  29.4 us (4%)
  between operations  14.3 us (2%)
    all_gather x7, blocking collectives, prefix_by_axis(): lax.all_gather(part.astype(kind), axis)  101 us
    all_to_all x1, waiting for transfers between devices, body(): lax.all_to_all(expert_output, SP, split_axis=0, concat_axis=0, tiled=True)  98.1 us
    all_to_all x2, blocking collectives, turned_blocks(): filled = lax.all_to_all(filled, axes[k], k, k, tiled=True)  97.9 us
    all_to_all x1, blocking collectives, gather_by_exchange(): return lax.all_to_all(copies, axis, dim, dim, tiled=True)  94.2 us
    all_to_all x1, blocking collectives, sent_and_summed(): lax.all_to_all(pieces, axis, split_axis=0, concat_axis=0, tiled=True)  65.9 us
    all_to_all x1, starting transfers between devices, body(): lax.all_to_all(expert_output, SP, split_axis=0, concat_axis=0, tiled=True)  29.9 us
  transfers between devices with their start and end apart: 3, of which 2 were waited for; matrix products, arithmetic and copies ran while one was open for 3% of the time, Pallas kernels for 0%

profile of v1, /device:TPU:33, one launch (start us, length us, event | category | flops | bytes accessed | tf_op | source)
XLA Modules:
  0.0 652.4 jit_solution(16418877423427005246)
XLA Ops:
  14.4 1.9 copy.218
  16.3 1.9 copy.219
  19.9 2.3 subtract_convert_fusion
  23.6 22.0 %all-gather = bf16[4,128,128]{2,1,0:T(8,128)(2,1)S(1)} all-gather(bf16[2,128,128]{2,1,0:T(8,128)(2,1)S(1)} %convolution_convert_fusion.1), channel_id=2, replica_groups=mesh['grp'=2,'sp_0'=16,'sp_1'=2,'tp'=4] {'sp_1'}, dimensions={0}, use_global_device_ids=true | all-gather | bytes 196608 | tf_op jit(solution)/shard_map/all_gather | solution.py:36
  45.6 1.8 all-gather.2
  48.9 1.2 reduce-window.24
  55.3 1.2 subtract_exponential_fusion
  56.5 1.7 multiply_subtract_fusion.1
  58.5 2.0 all-gather.1
  60.4 1.8 all-gather.4
  62.4 32.0 %all_gather.45 = bf16[16,4,64,64]{3,2,1,0:T(8,128)(2,1)S(1)} all-gather(bf16[1,4,64,64]{3,2,1,0:T(8,128)(2,1)S(1)} %fusion.70), channel_id=1, replica_groups=mesh['grp'=2,'sp_0'=16,'sp_1'=2,'tp'=4] {'sp_0'}, dimensions={0}, use_global_device_ids=true | all-gather | bytes 557056 | tf_op jit(solution)/shard_map/all_gather | solution.py:36
  94.4 20.6 %all-gather.5 = bf16[16,1,4]{2,1,0:T(2,128)(2,1)S(1)} all-gather(bf16[1,1,4]{2,1,0:T(2,128)(2,1)S(1)} %get-tuple-element.65), channel_id=1, replica_groups=mesh['grp'=2,'sp_0'=16,'sp_1'=2,'tp'=4] {'sp_0'}, dimensions={0}, use_global_device_ids=true | all-gather | bytes 136 | tf_op jit(solution)/shard_map/all_gather | solution.py:36
  115.7 20.7 %all-gather.3 = bf16[16,1,2]{2,1,0:T(2,128)(2,1)S(1)} all-gather(bf16[1,1,2]{2,1,0:T(2,128)(2,1)} %get-tuple-element.68), channel_id=1, replica_groups=mesh['grp'=2,'sp_0'=16,'sp_1'=2,'tp'=4] {'sp_0'}, dimensions={0}, use_global_device_ids=true | all-gather | bytes 68 | tf_op jit(solution)/shard_map/all_gather | solution.py:36
  137.8 4.1 fusion.31
  141.9 1.8 fusion.327
  144.1 3.1 fusion.34
  147.2 2.5 fusion.326
  149.8 2.0 fusion.328
  151.9 2.0 add_convert_fusion
  153.9 4.7 all-to-all-start
  160.2 1.4 scatter_custom_fusion
  161.7 12.3 %all-to-all-done = bf16[4,128,2048]{2,1,0:T(8,128)(2,1)} async-done(((bf16[4,128,2048]{2,1,0:T(8,128)(2,1)}), bf16[4,128,2048]{2,1,0:T(8,128)(2,1)}, u32[]{:S(2)}, u32[]{:S(2)}) %all-to-all-start) | async-done | bytes 2097184 | tf_op jit(solution)/shard_map/all_to_all | solution.py:59
  173.9 2.1 convert_reduce_fusion
  177.4 3.1 gather_fusion
  180.5 3.6 reshape_reshape_reshape.3
  184.1 2.5 copy.203
  186.6 24.8 %all_to_all.30 = bf16[16,2,1,12,2048]{4,0,3,2,1:T(8,128)(2,1)S(1)} all-to-all(bf16[16,2,1,12,2048]{4,0,3,2,1:T(8,128)(2,1)S(1)} %copy.203), channel_id=1, replica_groups=mesh['grp'=2,'sp_0'=16,'sp_1'=2,'tp'=4] {'sp_1'}, dimensions={1} | all-to-all | bytes 3145728 | tf_op jit(solution)/shard_map/all_to_all | solution.py:73
  211.3 1.6 copy.204
  213.0 73.1 %all_to_all.31 = bf16[16,2,1,12,2048]{4,1,3,2,0:T(2,128)(2,1)S(1)} all-to-all(bf16[16,2,1,12,2048]{4,1,3,2,0:T(2,128)(2,1)S(1)} %copy.204), channel_id=1, replica_groups=mesh['grp'=2,'sp_0'=16,'sp_1'=2,'tp'=4] {'sp_0'}, dimensions={0} | all-to-all | bytes 3145728 | tf_op jit(solution)/shard_map/all_to_all | solution.py:73
  286.0 2.6 copy.205
  288.6 3.6 reshape_reshape.4
  292.3 4.8 pad_maximum_fusion
  297.1 6.8 %copy.206 = bf16[128,12,2048]{2,1,0:T(8,128)(2,1)} copy(bf16[128,12,2048]{2,0,1:T(8,128)(2,1)S(1)} %pad_maximum_fusion) | data formatting | bytes 12582912 | tf_op jit(solution)/shard_map/concatenate | solution.py:20
  304.0 94.2 %all_to_all.32 = bf16[128,12,2048]{2,1,0:T(8,128)(2,1)} all-to-all(bf16[128,12,2048]{2,1,0:T(8,128)(2,1)} %copy.206), channel_id=1, replica_groups=mesh['grp'=2,'sp_0'=16,'sp_1'=2,'tp'=4] {'tp'}, dimensions={0} | all-to-all | bytes 12582912 | tf_op jit(solution)/shard_map/all_to_all | solution.py:21
  398.2 10.7 %reshape.746 = bf16[1536,2048]{1,0:T(8,128)(2,1)} reshape(bf16[128,12,2048]{2,1,0:T(8,128)(2,1)} %all_to_all.32) | data formatting | bytes 12582912 | tf_op jit(solution)/shard_map/reshape | solution.py:217
  408.9 6.3 convolution_minimum_fusion
  415.2 5.0 fusion.7
  420.2 3.6 dot_general.53
  423.8 6.1 convert_bitcast_fusion
  429.9 65.9 %all_to_all.33 = bf16[4,1,32,12,2048]{4,2,3,1,0:T(8,128)(2,1)S(1)} all-to-all(bf16[4,1,32,12,2048]{4,2,3,1,0:T(8,128)(2,1)S(1)} %convert_bitcast_fusion), channel_id=1, replica_groups=mesh['grp'=2,'sp_0'=16,'sp_1'=2,'tp'=4] {'tp'}, dimensions={0} | all-to-all | bytes 12582912 | tf_op jit(solution)/shard_map/all_to_all | solution.py:59
  495.8 1.2 bitcast_reduce_fusion
  497.0 2.2 copy.210
  499.2 29.9 %all-to-all-start.5 = ((bf16[32,12,2048]{2,1,0:T(8,128)(2,1)}), bf16[32,12,2048]{2,1,0:T(8,128)(2,1)}, u32[]{:S(2)}, u32[]{:S(2)}) async-start(bf16[32,12,2048]{2,1,0:T(8,128)(2,1)} %copy.210), calls=%async_computation.5 | async-start | bytes 4194304 | tf_op jit(solution)/shard_map/all_to_all | solution.py:229
  529.3 98.1 %all-to-all-done.5 = bf16[32,12,2048]{2,1,0:T(8,128)(2,1)} async-done(((bf16[32,12,2048]{2,1,0:T(8,128)(2,1)}), bf16[32,12,2048]{2,1,0:T(8,128)(2,1)}, u32[]{:S(2)}, u32[]{:S(2)}) %all-to-all-start.5) | async-done | bytes 1572896 | tf_op jit(solution)/shard_map/all_to_all | solution.py:229
  627.4 3.6 reshape.748
  631.0 4.9 gather_fusion.1
  635.9 3.5 reshape.793
  639.4 4.9 multiply_reduce_fusion
  (142 shorter events, 24.1 us)
Async XLA Ops:
  6.5 417.3 %copy-start = (bf16[1,512,2048]{2,1,0:T(8,128)(2,1)S(1)}, bf16[1,512,2048]{2,1,0:T(8,128)(2,1)}, u32[]{:S(2)}) copy-start(bf16[1,512,2048]{2,1,0:T(8,128)(2,1)} %param.33) | copy-start | bytes 6291460
  6.6 137.5 %all-gather.8.cloned.1.call-start = ((), (), s32[]{:S(2)}) async-start(), calls=%async_computation.6 | async-start | bytes 1114112 | tf_op jit(solution)/shard_map/all_gather | solution.py:36
  8.4 0.6 copy-start.21
  18.3 4.8 copy-start.31
  19.9 29.0 %copy-start.18 = (f32[512,4]{0,1:T(4,128)S(1)}, f32[512,4]{0,1:T(4,128)}, u32[]{:S(2)}) copy-start(f32[512,4]{0,1:T(4,128)} %param.24) | copy-start | bytes 24580
  22.2 31.8 %copy-start.7 = (bf16[512,256]{1,0:T(8,128)(2,1)S(1)}, bf16[512,256]{1,0:T(8,128)(2,1)}, u32[]{:S(2)}) copy-start(bf16[512,256]{1,0:T(8,128)(2,1)} %param.22) | copy-start | bytes 786436
  22.4 0.7 copy-start.10
  47.5 1.4 copy-start.23
  48.1 0.8 copy-start.26
  48.1 2.4 copy-start.25
  50.6 0.7 copy-start.15
  54.0 83.8 %copy-start.16 = (f32[1,4,4,128]{3,1,2,0:T(4,128)S(1)}, f32[1,4,4,128]{3,1,2,0:T(4,128)}, u32[]{:S(2)}) copy-start(f32[1,4,4,128]{3,1,2,0:T(4,128)} %copy-done.15) | copy-start | bytes 24580
  55.2 3.0 copy-start.13
  55.3 5.2 copy-start.32
  58.2 4.0 copy-start.11
  58.2 4.1 copy-start.12
  62.3 75.5 %copy-start.27 = (f32[4]{0:T(128)}, f32[4]{0:T(128)S(1)}, u32[]{:S(2)}) copy-start(f32[4]{0:T(128)S(1)} %get-tuple-element.66) | copy-start | bytes 52
  62.3 75.5 %copy-start.28 = (f32[4]{0:T(128)}, f32[4]{0:T(128)S(1)}, u32[]{:S(2)}) copy-start(f32[4]{0:T(128)S(1)} %get-tuple-element.67) | copy-start | bytes 52
  137.8 4.1 copy-start.14
  141.9 2.0 copy-start.24
  141.9 2.2 copy-start.20
  143.8 3.4 copy-start.8
  143.8 3.4 copy-start.9
  143.8 3.4 copy-start.22
  149.8 2.1 copy-start.6
  153.9 4.7 copy-start.19
  153.9 22.1 %copy-start.4 = (bf16[128,2048]{1,0:T(8,128)(2,1)S(1)}, bf16[128,2048]{1,0:T(8,128)(2,1)}, u32[]{:S(2)}) copy-start(bf16[128,2048]{1,0:T(8,128)(2,1)} %param.25) | copy-start | bytes 1572868
  153.9 20.0 %all-to-all-start = ((bf16[4,128,2048]{2,1,0:T(8,128)(2,1)}), bf16[4,128,2048]{2,1,0:T(8,128)(2,1)}, u32[]{:S(2)}, u32[]{:S(2)}) async-start(bf16[4,128,2048]{2,1,0:T(8,128)(2,1)} %bitcast.468), calls=%async_computation | async-start | bytes 4194304 | tf_op jit(solution)/shard_map/all_to_all | solution.py:59
  158.6 18.5 %copy-start.17 = (f32[2048]{0:T(1024)S(1)}, f32[2048]{0:T(1024)}, u32[]{:S(2)}) copy-start(f32[2048]{0:T(1024)} %param.28) | copy-start | bytes 24580
  176.1 1.0 copy-start.1
  408.9 6.3 copy-start.3
  408.9 6.3 copy-start.30
  497.0 32.1 %copy-start.29 = (f32[128,2]{0,1:T(2,128)S(1)}, f32[128,2]{0,1:T(2,128)}, u32[]{:S(2)}) copy-start(f32[128,2]{0,1:T(2,128)} %param.30) | copy-start | bytes 3076
  499.2 128.2 %all-to-all-start.5 = ((bf16[32,12,2048]{2,1,0:T(8,128)(2,1)}), bf16[32,12,2048]{2,1,0:T(8,128)(2,1)}, u32[]{:S(2)}, u32[]{:S(2)}) async-start(bf16[32,12,2048]{2,1,0:T(8,128)(2,1)} %copy.210), calls=%async_computation.5 | async-start | bytes 4194304 | tf_op jit(solution)/shard_map/all_to_all | solution.py:229
  635.9 8.4 %copy-start.2 = (f32[128,2048]{1,0:T(8,128)S(1)}, f32[128,2048]{1,0:T(8,128)}, u32[]{:S(2)}) copy-start(f32[128,2048]{1,0:T(8,128)} %copy-done.1) | copy-start | bytes 3145732
  639.4 4.9 copy-start.5
Sparse Core Ops, SparseCore 0:
  49.0 54.4 all-gather.7
